TPU v7x, 32 devices: a whole 2x2x4 slice. The times are simulated.
32 devices in a mesh: rep: 2 (over y), fs: 4 (over z), tp: 4 (over x, core).
Axes of the slice: x: 2, y: 2, z: 4, core: 2. Of those that a mesh axis runs over, the one named last changes fastest.
Arguments:
- tokens: bfloat16 [4096, 2048], P(('rep', 'fs'), 'tp'), may hold values from -6 to 6
- outer_gate: float32 [2048, 512], P('fs', 'tp'), may hold values from -0.125 to 0.125
- inner_gate: float32 [2048, 512], P('fs', 'tp'), may hold values from -0.125 to 0.125
- mixer_value: float32 [2048, 512], P('fs', 'tp'), may hold values from -0.125 to 0.125
- mixer_scales: float32 [3, 512], P(None, 'tp'), may hold values from 0.5 to 2
- mixer_taps: float32 [3, 512], P(None, 'tp'), may hold values from -3.5 to 3.5
- mixer_out: float32 [512, 2048], P('fs', 'tp'), may hold values from -0.25 to 0.25
- out_scale: float32 [2048], P('tp'), may hold values from 0.3 to 3
- first_gain: float32 [2048], replicated, may hold values from 0.1 to 1.9
- first_shift: float32 [2048], replicated, may hold values from -2 to 2
- up_proj: float32 [2048, 3072], P('fs', 'tp'), may hold values from -0.125 to 0.125
- gate_proj: float32 [2048, 3072], P('fs', 'tp'), may hold values from -0.125 to 0.125
- up_scales: float32 [2, 3072], P(None, 'tp'), may hold values from 0.5 to 2
- ffn_taps: float32 [3, 2, 3072], P(None, None, 'tp'), may hold values from -3.5 to 3.5
- ffn_shift: float32 [2, 3072], P(None, 'tp'), may hold values from -3 to 3
- down_proj: float32 [3072, 2048], P('fs', 'tp'), may hold values from -0.109375 to 0.109375
- down_scale: float32 [2048], P('tp'), may hold values from 0.3 to 3
- second_gain: float32 [2048], replicated, may hold values from 0.1 to 1.9
- second_shift: float32 [2048], replicated, may hold values from -2 to 2
Outputs:
- layer_out: bfloat16 [4096, 2048], P(('rep', 'fs'), 'tp')
All inputs are finite; a program needn't handle non-finite values.
Results may differ from a plain program's by a relative error of at most 0.017.
Values may be sent and summed in bfloat16 or wider, within the bound.
A program may use at most 64 MiB of HBM per device.

v0:
```python
import jax
import jax.numpy as jnp
from jax import lax
from jax.sharding import PartitionSpec as P

LEN = 128


norm_eps = 1e-05
residual_weight = 8.0**0.25


def causal_mix(signal, kernel_taps):
    sequences = signal.reshape(-1, LEN, signal.shape[-1])
    padded = jnp.pad(sequences, ((0, 0), (2, 0), (0, 0)))
    mixed = (
        kernel_taps[0] * padded[:, :-2]
        + kernel_taps[1] * padded[:, 1:-1]
        + kernel_taps[2] * padded[:, 2:]
    )
    return mixed.reshape(signal.shape)


def lowered(matrix):
    return matrix.astype(jnp.bfloat16)


def single_fold(operand, portion):
    return jnp.dot(operand, portion, preferred_element_type=jnp.float32)


def fold_step(operand, pieces):
    result = []
    for number in range(len(pieces)):
        result.append(jnp.dot(operand, pieces[number], preferred_element_type=jnp.float32))
    return tuple(result)


def own_columns(vector, own_width):
    return lax.dynamic_slice_in_dim(vector, lax.axis_index("tp") * own_width, own_width, 0)


def scaled_norm(summed, average, spread, gain_vector, shift_vector):
    return (summed - average) * lax.rsqrt(spread + norm_eps) * gain_vector + shift_vector


def local(
    tokens,
    outer_gate,
    inner_gate,
    mixer_value,
    mixer_scales,
    mixer_taps,
    mixer_out,
    out_scale,
    first_gain,
    first_shift,
    up_proj,
    gate_proj,
    up_scales,
    ffn_taps,
    ffn_shift,
    down_proj,
    down_scale,
    second_gain,
    second_shift,
):
    own_width = tokens.shape[1]
    full_width = own_width * lax.axis_size("tp")
    token_whole = lax.all_gather(tokens, "tp", axis=1, tiled=True)
    outer_part, inner_part, value_part = fold_step(
        token_whole,
        (
            lax.all_gather(lowered(outer_gate), "fs", axis=0, tiled=True),
            lax.all_gather(lowered(inner_gate), "fs", axis=0, tiled=True),
            lax.all_gather(lowered(mixer_value), "fs", axis=0, tiled=True),
        ),
    )
    outer_part = (outer_part * mixer_scales[0]).astype(jnp.bfloat16)
    inner_part = (inner_part * mixer_scales[1]).astype(jnp.bfloat16)
    value_part = (value_part * mixer_scales[2]).astype(jnp.bfloat16)
    product = inner_part.astype(jnp.float32) * value_part.astype(jnp.float32)
    mixed_conv = (outer_part.astype(jnp.float32) * causal_mix(product, mixer_taps)).astype(
        jnp.bfloat16
    )
    conv_whole = lax.all_gather(mixed_conv, "tp", axis=1, tiled=True)
    mixer_sum = (
        single_fold(conv_whole, lax.all_gather(lowered(mixer_out), "fs", axis=0, tiled=True))
        * out_scale
    )
    first_sum = residual_weight * tokens.astype(jnp.float32) + mixer_sum
    row_total, row_square = lax.psum(
        (jnp.sum(first_sum, 1, keepdims=True), jnp.sum(first_sum * first_sum, 1, keepdims=True)),
        "tp",
    )
    average = row_total / full_width
    spread = row_square / full_width - average * average
    normed = scaled_norm(
        first_sum,
        average,
        spread,
        own_columns(first_gain, own_width),
        own_columns(first_shift, own_width),
    ).astype(jnp.bfloat16)
    normed_whole = lax.all_gather(normed, "tp", axis=1, tiled=True)
    up_matrix, gate_matrix = (
        lax.all_gather(lowered(up_proj), "fs", axis=0, tiled=True),
        lax.all_gather(lowered(gate_proj), "fs", axis=0, tiled=True),
    )
    up_linear = jnp.dot(normed_whole, up_matrix, preferred_element_type=jnp.float32)
    gate_linear = jnp.dot(normed_whole, gate_matrix, preferred_element_type=jnp.float32)
    up_linear = up_linear * up_scales[0]
    gate_linear = gate_linear * up_scales[1]
    up_mixed = causal_mix(up_linear, ffn_taps[:, 0]) + ffn_shift[0]
    gate_mixed = causal_mix(gate_linear, ffn_taps[:, 1]) + ffn_shift[1]
    hidden = (up_mixed * jax.nn.silu(gate_mixed)).astype(jnp.bfloat16)
    hidden_whole = lax.all_gather(hidden, "tp", axis=1, tiled=True)
    ffn_sum = (
        single_fold(hidden_whole, lax.all_gather(lowered(down_proj), "fs", axis=0, tiled=True))
        * down_scale
    )
    second_sum = residual_weight * normed.astype(jnp.float32) + ffn_sum
    second_total, second_square = lax.psum(
        (jnp.sum(second_sum, 1, keepdims=True), jnp.sum(second_sum * second_sum, 1, keepdims=True)),
        "tp",
    )
    second_average = second_total / full_width
    second_spread = second_square / full_width - second_average * second_average
    return scaled_norm(
        second_sum,
        second_average,
        second_spread,
        own_columns(second_gain, own_width),
        own_columns(second_shift, own_width),
    ).astype(jnp.bfloat16)


def solution(mesh):
    return jax.shard_map(
        local,
        mesh=mesh,
        in_specs=(
            P(("rep", "fs"), "tp"),
            P("fs", "tp"),
            P("fs", "tp"),
            P("fs", "tp"),
            P(None, "tp"),
            P(None, "tp"),
            P("fs", "tp"),
            P("tp"),
            P(),
            P(),
            P("fs", "tp"),
            P("fs", "tp"),
            P(None, "tp"),
            P(None, None, "tp"),
            P(None, "tp"),
            P("fs", "tp"),
            P("tp"),
            P(),
            P(),
        ),
        out_specs=P(("rep", "fs"), "tp"),
        check_vma=False,
    )
```

profile of v0, /device:TPU:0, one launch (start us, length us, event | category | flops | bytes accessed | tf_op | source)
XLA Modules:
  0.0 314.0 jit_solution(7180715300881190758)
XLA Ops:
  6.5 0.7 all-gather.7.cloned.1.call-update
  7.3 0.0 copy-start.2
  7.3 0.0 copy-start.6
  7.3 0.0 all-gather.11.cloned.1.call-start
  7.3 2.4 convert_element_type.76
  9.8 0.0 all-gather.11.cloned.1.call-update
  9.8 0.0 all-gather.9.cloned.1.call-start
  9.9 1.0 copy.22
  11.0 0.0 copy-start.13
  11.0 0.0 copy-start.14
  11.0 0.8 dynamic_slice.12
  11.8 0.8 dynamic_slice.13
  12.5 17.4 %all_gather.36 = bf16[2048,128]{1,0:T(8,128)(2,1)S(1)} all-gather(bf16[512,128]{1,0:T(8,128)(2,1)S(1)} %convert_element_type.69), channel_id=1, replica_groups=mesh['rep'=2,'fs'=4,'tp'=4] {'fs'}, dimensions={0}, use_global_device_ids=true | all-gather | bytes 655360 | tf_op jit(solution)/shard_map/all_gather | solution.py:76
  29.9 16.9 %all_gather.35 = bf16[2048,128]{1,0:T(8,128)(2,1)S(1)} all-gather(bf16[512,128]{1,0:T(8,128)(2,1)S(1)} %convert_element_type.66), channel_id=1, replica_groups=mesh['rep'=2,'fs'=4,'tp'=4] {'fs'}, dimensions={0}, use_global_device_ids=true | all-gather | bytes 655360 | tf_op jit(solution)/shard_map/all_gather | solution.py:75
  46.8 22.6 %all_gather.34 = bf16[2048,128]{1,0:T(8,128)(2,1)S(1)} all-gather(bf16[512,128]{1,0:T(8,128)(2,1)S(1)} %convert_element_type.63), channel_id=1, replica_groups=mesh['rep'=2,'fs'=4,'tp'=4] {'fs'}, dimensions={0}, use_global_device_ids=true | all-gather | bytes 655360 | tf_op jit(solution)/shard_map/all_gather | solution.py:74
  69.4 20.2 %all_gather.38 = bf16[512,512]{1,0:T(8,128)(2,1)S(1)} all-gather(bf16[128,512]{1,0:T(8,128)(2,1)S(1)} %convert_element_type.73), channel_id=1, replica_groups=mesh['rep'=2,'fs'=4,'tp'=4] {'fs'}, dimensions={0}, use_global_device_ids=true | all-gather | bytes 655360 | tf_op jit(solution)/shard_map/all_gather | solution.py:88
  89.6 0.0 all-gather.7.cloned.1.call-done
  89.6 0.0 copy-start
  89.6 2.5 fusion.20
  92.1 0.7 fusion.18
  92.8 0.1 fusion.23
  92.9 0.0 copy-start.5
  92.9 0.0 copy-start.15
  92.9 0.7 fusion.15
  93.7 7.0 %all_gather.37 = bf16[512,512]{1,0:T(8,128)(2,1)S(1)} all-gather(bf16[512,128]{1,0:T(8,128)(2,1)S(1)} %fusion.15), channel_id=1, replica_groups=mesh['rep'=2,'fs'=4,'tp'=4] {'tp'}, dimensions={1}, use_global_device_ids=true | all-gather | bytes 655360 | tf_op jit(solution)/shard_map/all_gather | solution.py:86
  100.7 0.0 copy-done.5
  100.7 0.6 fusion.26
  101.3 0.0 copy-start.3
  101.3 7.0 %all-reduce.4 = (f32[512,1]{0,1:T(1,128)S(1)}, f32[512,1]{0,1:T(1,128)S(1)}) all-reduce(f32[512,1]{0,1:T(1,128)S(1)} %bitcast.57, f32[512,1]{0,1:T(1,128)S(1)} %bitcast.56), channel_id=1, replica_groups=mesh['rep'=2,'fs'=4,'tp'=4] {'tp'}, use_global_device_ids=true, to_apply=%region_3.4 | all-reduce | flops 1024 | bytes 8192 | tf_op jit(solution)/shard_map/psum | solution.py:92
  108.3 1.0 add_convert_fusion.1
  109.3 0.0 all-gather.9.cloned.1.call-update
  109.3 0.0 copy-start.4
  109.3 0.0 all-gather.13.cloned.1.call-start
  109.4 1.0 convert_element_type.77
  110.4 0.0 all-gather.13.cloned.1.call-update
  110.4 0.0 copy-start.11
  110.4 0.0 copy-start.12
  110.4 0.0 copy-start.10
  110.5 0.0 all-gather.17.cloned.1.call-start
  110.5 0.5 copy-done.4
  111.0 1.0 convert_element_type.79
  112.0 0.0 all-gather.17.cloned.1.call-update
  112.0 0.0 all-gather.15.cloned.1.call-start
  112.1 0.0 copy-done.12
  112.1 0.0 copy-done.10
  112.1 0.1 slice_reduce_fusion.4
  112.2 2.2 all-gather.11.cloned.1.call-done
  114.4 23.7 %all-gather.9.cloned.1.call-done = bf16[512,2048]{0,1:T(8,128)(2,1)} async-done(((bf16[512,512]{0,1:T(8,128)(2,1)}), bf16[512,2048]{0,1:T(8,128)(2,1)}) %all-gather.9.cloned.1.call-update) | async-done | bytes 2097168 | tf_op jit(solution)/shard_map/all_gather | solution.py:105
  138.2 4.4 %convolution_multiply_fusion.1 = f32[512,768]{1,0:T(8,128)S(1)} fusion(bf16[512,2048]{0,1:T(8,128)(2,1)} %all-gather.9.cloned.1.call-done, bf16[2048,768]{1,0:T(8,128)(2,1)} %all-gather.11.cloned.1.call-done, f32[768]{0:T(1024)S(1)} %get-tuple-element.18), kind=kOutput, calls=%fused_computation.17 | convolution fusion | flops 1611005952 | bytes 6818816 | tf_op jit(solution)/shard_map/dot_general | solution.py:110
  142.5 60.5 %all-gather.13.cloned.1.call-done = bf16[2048,768]{1,0:T(8,128)(2,1)} async-done(((bf16[512,768]{1,0:T(8,128)(2,1)}), bf16[2048,768]{1,0:T(8,128)(2,1)}) %all-gather.13.cloned.1.call-update) | async-done | bytes 3145744 | tf_op jit(solution)/shard_map/all_gather | solution.py:108
  203.1 4.4 %convolution_multiply_fusion = f32[512,768]{1,0:T(8,128)S(1)} fusion(bf16[512,2048]{0,1:T(8,128)(2,1)} %all-gather.9.cloned.1.call-done, bf16[2048,768]{1,0:T(8,128)(2,1)} %all-gather.13.cloned.1.call-done, f32[768]{0:T(1024)S(1)} %get-tuple-element.17), kind=kOutput, calls=%fused_computation.16 | convolution fusion | flops 1611005952 | bytes 6818816 | tf_op jit(solution)/shard_map/dot_general | solution.py:111
  207.4 0.9 fusion.2
  208.4 0.0 copy-start.1
  208.4 0.0 copy-start.16
  208.4 1.4 fusion.9
  209.8 0.0 all-gather.15.cloned.1.call-update
  209.8 0.8 dynamic_slice.14
  210.5 0.8 dynamic_slice.15
  211.3 55.3 %all-gather.17.cloned.1.call-done = bf16[3072,512]{1,0:T(8,128)(2,1)} async-done(((bf16[768,512]{1,0:T(8,128)(2,1)}), bf16[3072,512]{1,0:T(8,128)(2,1)}) %all-gather.17.cloned.1.call-update) | async-done | bytes 3145744 | tf_op jit(solution)/shard_map/all_gather | solution.py:119
  266.6 28.6 %all-gather.15.cloned.1.call-done = bf16[512,3072]{1,0:T(8,128)(2,1)} async-done(((bf16[512,768]{1,0:T(8,128)(2,1)}), bf16[512,3072]{1,0:T(8,128)(2,1)}) %all-gather.15.cloned.1.call-update) | async-done | bytes 3145744 | tf_op jit(solution)/shard_map/all_gather | solution.py:117
  295.2 4.8 %fusion.25 = (f32[512]{0:T(512)S(1)}, f32[512]{0:T(512)S(1)}, f32[512,512]{0,1:T(8,128)S(1)}) fusion(f32[512]{0:T(512)S(1)} %copy-done.16, bf16[512,3072]{1,0:T(8,128)(2,1)} %all-gather.15.cloned.1.call-done, bf16[3072,512]{1,0:T(8,128)(2,1)} %all-gather.17.cloned.1.call-done, bf16[512,512]{0,1:T(8,128)(2,1)S(1)} %copy-done.1), kind=kOutput, calls=%fused_computation.64 | convolution fusion | flops 1612446720 | bytes 7870464 | tf_op jit(solution)/shard_map/dot_general | solution.py:29
  300.0 5.9 %all-reduce.3 = (f32[512,1]{0,1:T(1,128)S(1)}, f32[512,1]{0,1:T(1,128)S(1)}) all-reduce(f32[512,1]{0,1:T(1,128)S(1)} %bitcast.59, f32[512,1]{0,1:T(1,128)S(1)} %bitcast.58), channel_id=1, replica_groups=mesh['rep'=2,'fs'=4,'tp'=4] {'tp'}, use_global_device_ids=true, to_apply=%region_7.8 | all-reduce | flops 1024 | bytes 8192 | tf_op jit(solution)/shard_map/psum | solution.py:123
  305.9 0.2 add_convert_fusion
  306.1 1.0 copy.23
  (27 shorter events, 0.2 us)
Async XLA Ops:
  6.5 83.1 %all-gather.7.cloned.1.call-start = ((), (), s32[]{:S(2)}) async-start(), calls=%async_computation | async-start | bytes 2621440 | tf_op jit(solution)/shard_map/all_gather | solution.py:70
  7.3 2.6 copy-start.2
  7.3 3.6 %copy-start.6 = (f32[512,128]{1,0:T(8,128)S(1)}, f32[512,128]{1,0:T(8,128)}, u32[]{:S(2)}) copy-start(f32[512,128]{1,0:T(8,128)} %param.22) | copy-start | bytes 786436
  7.3 107.2 %all-gather.11.cloned.1.call-start = ((), (), s32[]{:S(2)}) async-start(), calls=%async_computation.2 | async-start | bytes 3932160 | tf_op jit(solution)/shard_map/all_gather | solution.py:107
  9.8 1.1 copy-start.7
  9.8 1.2 copy-start.8
  9.8 1.2 copy-start.9
  9.8 128.4 %all-gather.9.cloned.1.call-start = ((), (), s32[]{:S(2)}) async-start(), calls=%async_computation.1 | async-start | bytes 2621440 | tf_op jit(solution)/shard_map/all_gather | solution.py:105
  11.0 78.6 %copy-start.13 = (f32[3,128]{1,0:T(4,128)S(1)}, f32[3,128]{1,0:T(4,128)}, u32[]{:S(2)}) copy-start(f32[3,128]{1,0:T(4,128)} %param.23) | copy-start | bytes 4612
  11.0 78.6 %copy-start.14 = (f32[3,128]{1,0:T(4,128)S(1)}, f32[3,128]{1,0:T(4,128)}, u32[]{:S(2)}) copy-start(f32[3,128]{1,0:T(4,128)} %param.24) | copy-start | bytes 4612
  89.6 2.5 copy-start
  92.9 7.8 %copy-start.5 = (bf16[512,512]{0,1:T(8,128)(2,1)S(1)}, bf16[512,512]{0,1:T(8,128)(2,1)}, u32[]{:S(2)}) copy-start(bf16[512,512]{0,1:T(8,128)(2,1)} %copy.22) | copy-start | bytes 1572868
  92.9 7.8 %copy-start.15 = (f32[512]{0:T(512)S(1)}, f32[512]{0:T(512)}, u32[]{:S(2)}) copy-start(f32[512]{0:T(512)} %param.26) | copy-start | bytes 6148
  101.3 8.1 %copy-start.3 = (f32[512,768]{1,0:T(8,128)S(1)}, f32[512,768]{1,0:T(8,128)}, u32[]{:S(2)}) copy-start(f32[512,768]{1,0:T(8,128)} %param.30) | copy-start | bytes 4718596
  109.3 1.7 copy-start.4
  109.3 93.8 %all-gather.13.cloned.1.call-start = ((), (), s32[]{:S(2)}) async-start(), calls=%async_computation.3 | async-start | bytes 3932160 | tf_op jit(solution)/shard_map/all_gather | solution.py:108
  110.4 1.6 copy-start.11
  110.4 1.7 copy-start.12
  110.4 1.7 copy-start.10
  110.5 156.2 %all-gather.17.cloned.1.call-start = ((), (), s32[]{:S(2)}) async-start(), calls=%async_computation.5 | async-start | bytes 3932160 | tf_op jit(solution)/shard_map/all_gather | solution.py:119
  112.0 183.2 %all-gather.15.cloned.1.call-start = ((), (), s32[]{:S(2)}) async-start(), calls=%async_computation.4 | async-start | bytes 3932160 | tf_op jit(solution)/shard_map/all_gather | solution.py:117
  208.4 86.8 %copy-start.1 = (bf16[512,512]{0,1:T(8,128)(2,1)S(1)}, bf16[512,512]{0,1:T(8,128)(2,1)}, u32[]{:S(2)}) copy-start(bf16[512,512]{0,1:T(8,128)(2,1)} %add_convert_fusion.1) | copy-start | bytes 1572868
  208.4 86.8 %copy-start.16 = (f32[512]{0:T(512)S(1)}, f32[512]{0:T(512)}, u32[]{:S(2)}) copy-start(f32[512]{0:T(512)} %param.35) | copy-start | bytes 6148
Sparse Core Ops, SparseCore 0:
  8.9 25.2 all-gather.6
  35.8 78.6 all-gather.10
  116.0 22.1 all-gather.8
  139.6 63.4 all-gather.12
  204.5 62.0 all-gather.16
  268.0 27.1 all-gather.14
where the time goes:
time: 314 us
  waiting for transfers between devices  171 us (54%)
  blocking collectives  96.9 us (31%)
  matrix products  18 us (6%)
  between operations  13.8 us (4%)
  other arithmetic  8.13 us (3%)
  local copies, waits for them, and re-layouts  5.76 us (2%)
    all_gather x1, waiting for transfers between devices, local(): lax.all_gather(lowered(gate_proj), 'fs', axis=0, tiled=True)  60.5 us
    all_gather x1, waiting for transfers between devices, local(): lax.all_gather(lowered(down_proj), 'fs', axis=0, tiled=True)  55.3 us
    all_gather x1, waiting for transfers between devices, local(): hidden_whole = lax.all_gather(hidden, 'tp', axis=1, tiled=True)  28.6 us
    all_gather x1, waiting for transfers between devices, local(): normed_whole = lax.all_gather(normed, 'tp', axis=1, tiled=True)  23.7 us
    all_gather x1, blocking collectives, local(): lax.all_gather(lowered(outer_gate), 'fs', axis=0, tiled=True)  22.6 us
    all_gather x1, blocking collectives, local(): lax.all_gather(lowered(mixer_out), 'fs', axis=0, tiled=True)  20.2 us
    all_gather x1, blocking collectives, local(): lax.all_gather(lowered(mixer_value), 'fs', axis=0, tiled=True)  17.4 us
    all_gather x1, blocking collectives, local(): lax.all_gather(lowered(inner_gate), 'fs', axis=0, tiled=True)  16.9 us
  transfers between devices with their start and end apart: 6, of which 5 were waited for; matrix products, arithmetic and copies ran while one was open for 8% of the time, Pallas kernels for 0%

commit v1 on v0

--- a/solution.py
+++ b/solution.py
@@ -1,6 +1,10 @@
+import functools
+
 import jax
 import jax.numpy as jnp
 from jax import lax
+from jax.experimental import pallas as pl
+from jax.experimental.pallas import tpu as pltpu
 from jax.sharding import PartitionSpec as P
 
 LEN = 128
@@ -135,9 +139,512 @@
     ).astype(jnp.bfloat16)
 
 
+LANES = 128
+
+
+def shifted_mix(signal, taps, first_tap):
+    rows = lax.broadcasted_iota(jnp.int32, signal.shape, 0) % LEN
+    one = jnp.where(rows >= 1, pltpu.roll(signal, 1, 0), 0.0)
+    two = jnp.where(rows >= 2, pltpu.roll(signal, 2, 0), 0.0)
+    return (
+        taps[first_tap : first_tap + 1] * two
+        + taps[first_tap + 1 : first_tap + 2] * one
+        + taps[first_tap + 2 : first_tap + 3] * signal
+    )
+
+
+def dot32(left, right):
+    return jnp.dot(left, right, preferred_element_type=jnp.float32)
+
+
+def kernel(
+    fs,
+    tp,
+    tokens_hbm,
+    outer_hbm,
+    inner_hbm,
+    value_hbm,
+    out_hbm,
+    up_hbm,
+    gate_hbm,
+    down_hbm,
+    narrow,
+    model,
+    wide,
+    result,
+    mix_f,
+    out_f,
+    up_f,
+    gate_f,
+    down_f,
+    mix_g,
+    out_g,
+    ug_g,
+    down_g,
+    token_all,
+    conv_all,
+    norm_all,
+    hidden_all,
+    first_sum,
+    total,
+    stats,
+    load_sem,
+    send_z,
+    send_y,
+    recv_z,
+    recv_y,
+    send_x,
+    recv_x,
+    send_s,
+    recv_s,
+):
+    r, z, t = lax.axis_index("rep"), lax.axis_index("fs"), lax.axis_index("tp")
+    sibling = t + 1 - 2 * (t % 2)
+    across = (t + 2) % tp
+    diagonal = (sibling + 2) % tp
+    other = 1 - r
+    rows, own_width = result.shape
+    full_width = own_width * tp
+    channels = conv_all.shape[2]
+    blocks = ug_g.shape[1]
+
+    sources = (tokens_hbm, outer_hbm, inner_hbm, value_hbm, out_hbm, up_hbm, gate_hbm, down_hbm)
+    places = (token_all.at[t], mix_f.at[0], mix_f.at[1], mix_f.at[2], out_f, up_f, gate_f, down_f)
+    loads = [
+        pltpu.make_async_copy(source, place, load_sem.at[number])
+        for number, (source, place) in enumerate(zip(sources, places))
+    ]
+    for load in loads:
+        load.start()
+
+    barrier = pltpu.get_barrier_semaphore()
+    for peer in (sibling, across, diagonal):
+        pl.semaphore_signal(barrier, inc=1, device_id={"tp": peer}, device_id_type=pl.DeviceIdType.MESH)
+    pl.semaphore_signal(barrier, inc=1, device_id={"rep": other}, device_id_type=pl.DeviceIdType.MESH)
+
+    @pl.when(z > 0)
+    def _():
+        pl.semaphore_signal(barrier, inc=1, device_id={"fs": z - 1}, device_id_type=pl.DeviceIdType.MESH)
+
+    @pl.when(z < fs - 1)
+    def _():
+        pl.semaphore_signal(barrier, inc=1, device_id={"fs": z + 1}, device_id_type=pl.DeviceIdType.MESH)
+
+    inside = (z > 0) & (z < fs - 1)
+
+    @pl.when(inside)
+    def _():
+        pl.semaphore_wait(barrier, 6)
+
+    @pl.when(jnp.logical_not(inside))
+    def _():
+        pl.semaphore_wait(barrier, 5)
+
+    def hop(number, slot, ref, peer, kind):
+        return pltpu.make_async_remote_copy(
+            src_ref=ref(slot),
+            dst_ref=ref(slot),
+            send_sem=send_x.at[number, kind],
+            recv_sem=recv_x.at[number, slot],
+            device_id={"tp": peer},
+            device_id_type=pl.DeviceIdType.MESH,
+        )
+
+    def exchange_start(number, ref):
+        hop(number, t, ref, across, 0).start()
+        hop(number, t, ref, sibling, 1).start()
+
+    def exchange_pass(number, ref):
+        hop(number, across, ref, across, 0).wait_recv()
+        hop(number, across, ref, sibling, 2).start()
+
+    def exchange_end(number, ref):
+        hop(number, sibling, ref, sibling, 1).wait_recv()
+        hop(number, diagonal, ref, sibling, 2).wait_recv()
+
+    def exchange_sent(number, ref):
+        hop(number, t, ref, across, 0).wait_send()
+        hop(number, t, ref, sibling, 1).wait_send()
+        hop(number, across, ref, sibling, 2).wait_send()
+
+    def token_block(slot):
+        return token_all.at[slot]
+
+    def conv_block(slot):
+        return conv_all.at[slot]
+
+    def norm_block(slot):
+        return norm_all.at[slot]
+
+    def hidden_block(number):
+        return lambda slot: hidden_all.at[slot, number]
+
+    def mix_unit(part):
+        size = mix_g.shape[1] // 4
+        return lambda source, half: mix_g.at[source, pl.ds(pl.multiple_of((part * 2 + half) * size, size), size)]
+
+    def out_unit(source, half):
+        size = out_g.shape[1] // 2
+        return out_g.at[source, pl.ds(pl.multiple_of(half * size, size), size)]
+
+    def ug_unit(block):
+        size = ug_g.shape[2] // 2
+        return lambda source, half: ug_g.at[source, block, pl.ds(pl.multiple_of(half * size, size), size)]
+
+    def down_unit(part):
+        size = LANES
+        return lambda source, half: down_g.at[source, pl.ds(pl.multiple_of((part * 2 + half) * size, size), size)]
+
+    units = [mix_unit(0), mix_unit(1), out_unit]
+    units += [ug_unit(block) for block in range(blocks)]
+    units += [down_unit(part) for part in range(blocks // 2)]
+    count = len(units)
+    first_ug, first_down = 3, 3 + blocks
+
+    def along(unit, source, target, way):
+        ref = units[unit](source, r)
+        return pltpu.make_async_remote_copy(
+            src_ref=ref,
+            dst_ref=ref,
+            send_sem=send_z.at[unit, source, way],
+            recv_sem=recv_z.at[unit, source],
+            device_id={"fs": target},
+            device_id_type=pl.DeviceIdType.MESH,
+        )
+
+    def over(unit, source, half):
+        ref = units[unit](source, half)
+        return pltpu.make_async_remote_copy(
+            src_ref=ref,
+            dst_ref=ref,
+            send_sem=send_y.at[unit, source],
+            recv_sem=recv_y.at[unit, source],
+            device_id={"rep": other},
+            device_id_type=pl.DeviceIdType.MESH,
+        )
+
+    def own(unit):
+        @pl.when(z < fs - 1)
+        def _():
+            along(unit, z, z + 1, 0).start()
+
+        @pl.when(z > 0)
+        def _():
+            along(unit, z, z - 1, 1).start()
+
+    def own_sent(unit):
+        @pl.when(z < fs - 1)
+        def _():
+            along(unit, z, z + 1, 0).wait_send()
+
+        @pl.when(z > 0)
+        def _():
+            along(unit, z, z - 1, 1).wait_send()
+
+    def passed(unit, distance, sent):
+        @pl.when(z >= distance)
+        def _():
+            source = z - distance
+            if not sent:
+                along(unit, source, z, 0).wait_recv()
+
+            @pl.when(z < fs - 1)
+            def _():
+                copy = along(unit, source, z + 1, 0)
+                copy.wait_send() if sent else copy.start()
+
+            copy = over(unit, source, r)
+            copy.wait_send() if sent else copy.start()
+
+        @pl.when(z + distance < fs)
+        def _():
+            source = z + distance
+            if not sent:
+                along(unit, source, z, 1).wait_recv()
+
+            @pl.when(z > 0)
+            def _():
+                copy = along(unit, source, z - 1, 1)
+                copy.wait_send() if sent else copy.start()
+
+            copy = over(unit, source, r)
+            copy.wait_send() if sent else copy.start()
+
+    def step(number):
+        if number < count:
+            own(number)
+        for distance in range(1, fs):
+            if 0 <= number - distance < count:
+                passed(number - distance, distance, False)
+
+    def need(unit):
+        for source in range(fs):
+
+            @pl.when(z != source)
+            def _():
+                over(unit, source, other).wait_recv()
+
+    def lower_block(block):
+        columns = slice(block * LANES, (block + 1) * LANES)
+        ug_g[z, block, :, :LANES] = up_f[:, columns].astype(jnp.bfloat16)
+        ug_g[z, block, :, LANES:] = gate_f[:, columns].astype(jnp.bfloat16)
+
+    def summing(number, peer, slot, kind):
+        return pltpu.make_async_remote_copy(
+            src_ref=stats.at[number, slot],
+            dst_ref=stats.at[number, slot],
+            send_sem=send_s.at[number, kind],
+            recv_sem=recv_s.at[number, slot],
+            device_id={"tp": peer},
+            device_id_type=pl.DeviceIdType.MESH,
+        )
+
+    def sums_start(number, summed):
+        lane = lax.broadcasted_iota(jnp.int32, (rows, LANES), 1)
+        one = jnp.sum(summed, axis=1, keepdims=True)
+        two = jnp.sum(summed * summed, axis=1, keepdims=True)
+        stats[number, t] = jnp.transpose(jnp.where(lane == 0, one, two))[:8]
+        for kind, peer in enumerate((across, diagonal, sibling)):
+            summing(number, peer, t, kind).start()
+
+    def sums_end(number):
+        for kind, peer in enumerate((across, diagonal, sibling)):
+            summing(number, peer, peer, kind).wait_recv()
+        whole = stats[number, 0]
+        for slot in range(1, tp):
+            whole = whole + stats[number, slot]
+        back = jnp.transpose(jnp.concatenate([whole] * (LANES // 8), axis=0))
+        average = back[:, 0:1] / full_width
+        return average, back[:, 1:2] / full_width - average * average
+
+    def mixer():
+        for unit in (0, 1):
+            need(unit)
+        exchange_end(0, token_block)
+        parts = dot32(token_all[0], mix_g[0])
+        for slot in range(1, tp):
+            parts = parts + dot32(token_all[slot], mix_g[slot])
+        scaled = [
+            (parts[:, part * channels : (part + 1) * channels] * narrow[part : part + 1])
+            .astype(jnp.bfloat16)
+            .astype(jnp.float32)
+            for part in range(3)
+        ]
+        mixed = scaled[0] * shifted_mix(scaled[1] * scaled[2], narrow, 3)
+        conv_all[t] = mixed.astype(jnp.bfloat16)
+        exchange_start(1, conv_block)
+
+    def mixer_output():
+        need(2)
+        exchange_end(1, conv_block)
+        summed = dot32(conv_all[0], out_g[0])
+        for slot in range(1, tp):
+            summed = summed + dot32(conv_all[slot], out_g[slot])
+        summed = summed * model[0:1] + residual_weight * token_all[t].astype(jnp.float32)
+        first_sum[...] = summed
+        sums_start(0, summed)
+
+    def first_norm():
+        average, spread = sums_end(0)
+        norm_all[t] = scaled_norm(first_sum[...], average, spread, model[1:2], model[2:3]).astype(jnp.bfloat16)
+        exchange_start(2, norm_block)
+
+    def hidden(block):
+        need(first_ug + block)
+        both = dot32(norm_all[0], ug_g[0, block])
+        for slot in range(1, tp):
+            both = both + dot32(norm_all[slot], ug_g[slot, block])
+        taps = wide[:, block * LANES : (block + 1) * LANES]
+        up_mixed = shifted_mix(both[:, :LANES] * taps[0:1], taps, 2) + taps[8:9]
+        gate_mixed = shifted_mix(both[:, LANES:] * taps[1:2], taps, 5) + taps[9:10]
+        hidden_all[t, block] = (up_mixed * gate_mixed / (1.0 + jnp.exp(-gate_mixed))).astype(jnp.bfloat16)
+        exchange_start(3 + block, hidden_block(block))
+
+    def down(part):
+        need(first_down + part)
+        for block in (2 * part, 2 * part + 1):
+            exchange_end(3 + block, hidden_block(block))
+        summed = None
+        for slot in range(tp):
+            left = jnp.concatenate([hidden_all[slot, 2 * part], hidden_all[slot, 2 * part + 1]], axis=1)
+            term = dot32(left, down_g[slot, part * 2 * LANES : (part + 1) * 2 * LANES])
+            summed = term if summed is None else summed + term
+        total[...] = summed if part == 0 else total[...] + summed
+
+    for load in loads[:4]:
+        load.wait()
+    exchange_start(0, token_block)
+    for part in range(3):
+        mix_g[z, :, part * channels : (part + 1) * channels] = mix_f[part].astype(jnp.bfloat16)
+    step(0)
+    step(1)
+    loads[4].wait()
+    out_g[z] = out_f[...].astype(jnp.bfloat16)
+    step(2)
+    exchange_pass(0, token_block)
+    loads[5].wait()
+    loads[6].wait()
+    loads[7].wait()
+    lower_block(0)
+    step(3)
+    lower_block(1)
+    step(4)
+    mixer()
+    lower_block(2)
+    step(5)
+    exchange_pass(1, conv_block)
+    mixer_output()
+    lower_block(3)
+    step(6)
+    first_norm()
+    lower_block(4)
+    step(7)
+    for block in range(5, blocks):
+        lower_block(block)
+    exchange_pass(2, norm_block)
+    step(8)
+    down_g[z] = down_f[...].astype(jnp.bfloat16)
+    exchange_end(2, norm_block)
+    hidden(0)
+    number = 9
+    ready = 1
+    moved = 0
+    while ready < blocks:
+        step(number)
+        number += 1
+        while moved < ready:
+            exchange_pass(3 + moved, hidden_block(moved))
+            moved += 1
+        while ready < blocks and first_ug + ready + fs - 1 <= number - 1:
+            hidden(ready)
+            ready += 1
+    for part in range(blocks // 2):
+        while number <= first_down + part + fs - 1:
+            step(number)
+            number += 1
+        while moved < blocks:
+            exchange_pass(3 + moved, hidden_block(moved))
+            moved += 1
+        down(part)
+
+    second = total[...] * model[3:4] + residual_weight * norm_all[t].astype(jnp.float32)
+    total[...] = second
+    sums_start(1, second)
+
+    for unit in range(count):
+        own_sent(unit)
+        for distance in range(1, fs):
+            passed(unit, distance, True)
+    refs = [token_block, conv_block, norm_block] + [hidden_block(block) for block in range(blocks)]
+    for place, ref in enumerate(refs):
+        exchange_sent(place, ref)
+    average, spread = sums_end(1)
+    result[...] = scaled_norm(total[...], average, spread, model[4:5], model[5:6]).astype(result.dtype)
+    for place in range(2):
+        for kind, peer in enumerate((across, diagonal, sibling)):
+            summing(place, peer, t, kind).wait_send()
+
+
+def fused(
+    fs,
+    tp,
+    tokens,
+    outer_gate,
+    inner_gate,
+    mixer_value,
+    mixer_scales,
+    mixer_taps,
+    mixer_out,
+    out_scale,
+    first_gain,
+    first_shift,
+    up_proj,
+    gate_proj,
+    up_scales,
+    ffn_taps,
+    ffn_shift,
+    down_proj,
+    down_scale,
+    second_gain,
+    second_shift,
+):
+    rows, own_width = tokens.shape
+    depth, channels = outer_gate.shape
+    hidden = up_proj.shape[1]
+    blocks = hidden // LANES
+    count = 3 + blocks + blocks // 2
+    narrow = jnp.concatenate([mixer_scales, mixer_taps], axis=0)
+    model = jnp.stack(
+        [
+            out_scale,
+            own_columns(first_gain, own_width),
+            own_columns(first_shift, own_width),
+            down_scale,
+            own_columns(second_gain, own_width),
+            own_columns(second_shift, own_width),
+        ]
+    )
+    wide = jnp.concatenate([up_scales, ffn_taps[:, 0], ffn_taps[:, 1], ffn_shift], axis=0)
+    any_space = pl.BlockSpec(memory_space=pl.ANY)
+    in_vmem = pl.BlockSpec(memory_space=pltpu.VMEM)
+    return pl.pallas_call(
+        functools.partial(kernel, fs, tp),
+        out_shape=jax.ShapeDtypeStruct((rows, own_width), jnp.bfloat16),
+        in_specs=[any_space] * 8 + [in_vmem] * 3,
+        out_specs=in_vmem,
+        scratch_shapes=[
+            pltpu.VMEM((3, depth, channels), jnp.float32),
+            pltpu.VMEM(mixer_out.shape, jnp.float32),
+            pltpu.VMEM(up_proj.shape, jnp.float32),
+            pltpu.VMEM(gate_proj.shape, jnp.float32),
+            pltpu.VMEM(down_proj.shape, jnp.float32),
+            pltpu.VMEM((fs, depth, 3 * channels), jnp.bfloat16),
+            pltpu.VMEM((fs,) + mixer_out.shape, jnp.bfloat16),
+            pltpu.VMEM((fs, blocks, depth, 2 * LANES), jnp.bfloat16),
+            pltpu.VMEM((fs,) + down_proj.shape, jnp.bfloat16),
+            pltpu.VMEM((tp, rows, own_width), jnp.bfloat16),
+            pltpu.VMEM((tp, rows, channels), jnp.bfloat16),
+            pltpu.VMEM((tp, rows, own_width), jnp.bfloat16),
+            pltpu.VMEM((tp, blocks, rows, LANES), jnp.bfloat16),
+            pltpu.VMEM((rows, own_width), jnp.float32),
+            pltpu.VMEM((rows, own_width), jnp.float32),
+            pltpu.VMEM((2, tp, 8, rows), jnp.float32),
+            pltpu.SemaphoreType.DMA((8,)),
+            pltpu.SemaphoreType.DMA((count, fs, 2)),
+            pltpu.SemaphoreType.DMA((count, fs)),
+            pltpu.SemaphoreType.DMA((count, fs)),
+            pltpu.SemaphoreType.DMA((count, fs)),
+            pltpu.SemaphoreType.DMA((3 + blocks, 3)),
+            pltpu.SemaphoreType.DMA((3 + blocks, tp)),
+            pltpu.SemaphoreType.DMA((2, 3)),
+            pltpu.SemaphoreType.DMA((2, tp)),
+        ],
+        compiler_params=pltpu.CompilerParams(
+            collective_id=0, has_side_effects=True, vmem_limit_bytes=60 * 1024 * 1024
+        ),
+    )(
+        tokens,
+        outer_gate,
+        inner_gate,
+        mixer_value,
+        mixer_out,
+        up_proj,
+        gate_proj,
+        down_proj,
+        narrow,
+        model,
+        wide,
+    )
+
+
+def fits(mesh):
+    return mesh.shape["rep"] == 2 and mesh.shape["fs"] == 4 and mesh.shape["tp"] == 4
+
+
 def solution(mesh):
+    body = functools.partial(fused, mesh.shape["fs"], mesh.shape["tp"]) if fits(mesh) else local
     return jax.shard_map(
-        local,
+        body,
         mesh=mesh,
         in_specs=(
             P(("rep", "fs"), "tp"),

time: 314 us -> 135 us (0.43)
  waiting for transfers between devices: 171 us -> 0 us
  Pallas kernels: 0 us -> 125 us
  blocking collectives: 96.9 us -> 0 us
  matrix products: 18 us -> 0 us
  between operations: 13.8 us -> 0.02 us
  other arithmetic: 8.13 us -> 2.64 us
    all_gather x6 -> x0, waiting for transfers between devices: 170 us -> none  [the longest x1 60.5 us: local(): lax.all_gather(lowered(gate_proj), 'fs', axis=0, tiled=True)]
    pallas_call x0 -> x1, Pallas kernels: none -> 125 us  [fused(): pl.pallas_call(functools.partial(kernel, fs, tp), out_shape=jax.ShapeDtyp...]
    all_gather x5 -> x0, blocking collectives: 84.1 us -> none  [the longest x1 22.6 us: local(): lax.all_gather(lowered(outer_gate), 'fs', axis=0, tiled=True)]
    dot_general x7 -> x0, matrix products: 18 us -> none  [the longest x2 5.36 us: single_fold(): return jnp.dot(operand, portion, preferred_element_type=jnp.float32)]
    psum x2 -> x0, blocking collectives: 12.8 us -> none  [the longest x1 6.95 us: local(): lax.psum((jnp.sum(first_sum, 1, keepdims=True), jnp.sum(first_sum * first...]
    convert_element_type x10 -> x0, other arithmetic: 7.1 us -> none  [the longest x7 4.51 us: lowered(): return matrix.astype(jnp.bfloat16)]
  transfers between devices with their start and end apart: 6 -> 0, of which waited for: 5 -> 0; matrix products, arithmetic and copies ran while one was open for 8% -> 0% of each run, Pallas kernels for 0% -> 0%
where the time goes in v1:
time: 135 us
  Pallas kernels  125 us (93%)
  local copies, waits for them, and re-layouts  7.05 us (5%)
  other arithmetic  2.64 us (2%)
    pallas_call x1, Pallas kernels, fused(): pl.pallas_call(functools.partial(kernel, fs, tp), out_shape=jax.ShapeDtyp...  125 us
    dynamic_slice x4, local copies, waits for them, and re-layouts, own_columns(): lax.dynamic_slice_in_dim(vector, lax.axis_index('tp') * own_width, own_wi...  3.04 us

profile of v1, /device:TPU:0, one launch (start us, length us, event | category | flops | bytes accessed | tf_op | source)
XLA Modules:
  0.0 134.8 jit_solution(2091710055497902113)
XLA Ops:
  0.0 0.8 dynamic_slice.12
  0.8 0.8 dynamic_slice.13
  1.5 0.8 dynamic_slice.14
  2.3 0.8 dynamic_slice.15
  3.0 1.3 pad_maximum_fusion.1.narrow
  4.3 1.3 stack.27.model
  5.7 0.8 fusion
  6.5 1.3 %pad_maximum_fusion.wide = f32[10,768]{1,0:T(8,128)} fusion(f32[2,768]{1,0:T(2,128)} %param.33, f32[3,768]{1,0:T(4,128)S(1)} %get-tuple-element.7, f32[3,768]{1,0:T(4,128)S(1)} %get-tuple-element.8, f32[2,768]{1,0:T(2,128)} %param.31), kind=kLoop, calls=%fused_computation | loop fusion | flops 23040 | bytes 61440 | tf_op jit(solution)/shard_map/concatenate | solution.py:587
  7.8 125.1 %shard_map.181 = bf16[512,512]{1,0:T(8,128)(2,1)} custom-call(bf16[512,512]{1,0:T(8,128)(2,1)} %tokens_hbm.1, f32[512,128]{1,0:T(8,128)} %outer_hbm.1, f32[512,128]{1,0:T(8,128)} %inner_hbm.1, f32[512,128]{1,0:T(8,128)} %value_hbm.1, f32[128,512]{1,0:T(8,128)} %out_hbm.1, f32[512,768]{1,0:T(8,128)} %up_hbm.1, f32[512,768]{1,0:T(8,128)} %gate_hbm.1, ...), custom_call_target="tpu_custom_call" | custom-call | tf_op jit(solution)/shard_map/pallas_call | solution.py:590
  132.9 1.9 %copy.27 = bf16[512,512]{1,0:T(8,128)(2,1)} copy(bf16[512,512]{1,0:T(8,128)(2,1)} %shard_map.181) | data formatting | bytes 1048576
  (1 shorter events, 0.0 us)
